TPU v7x, 32 devices: a whole 2x2x4 slice. The times are simulated.
32 devices in a mesh: sp: 8 (over z, x), dp: 4 (over y, core).
Axes of the slice: x: 2, y: 2, z: 4, core: 2. Of those that a mesh axis runs over, the one named last changes fastest.
Arguments:
- resid: bfloat16 [4, 1024, 2048], P('dp', 'sp'), may hold values from -6 to 6
- queries: bfloat16 [4, 1024, 2048], P('dp', 'sp'), may hold values from -7 to 7
- keys: bfloat16 [4, 1024, 2048], P('dp', 'sp'), may hold values from -7 to 7
- values: bfloat16 [4, 1024, 2048], P('dp', 'sp'), may hold values from -6 to 6
- forget_cache: float32 [4, 32, 1024], P('dp', 'sp'), may hold values from -131 to 0, as said below
- query_gain: float32 [64], replicated, may hold values from 0.5 to 8
- key_gain: float32 [64], replicated, may hold values from 0.5 to 8
- out_weight: bfloat16 [2048, 2048], P(None, 'dp'), may hold values from -0.125 to 0.125
- norm_gain: float32 [2048], replicated, may hold values from 0.1 to 1.9
- routes: int32 [4, 1024, 2], P('dp', 'sp'), may hold values from 0 to 31, all different within a row; in each aligned block of 128 rows (0 to 127, 128 to 255, ..., all dimensions but the last counted through in order) at most 16 rows name the same one
- group_weight: float32 [4, 1024], P('dp', 'sp'), may hold values from 0.2 to 1
- inner_share: float32 [4, 1024, 2], P('dp', 'sp'), may hold values from 0.1 to 1
- expert_gate: bfloat16 [32, 2048, 1024], P(('sp', 'dp')), may hold values from -0.125 to 0.125
- expert_up: bfloat16 [32, 2048, 1024], P(('sp', 'dp')), may hold values from -0.125 to 0.125
- expert_down: bfloat16 [32, 1024, 2048], P(('sp', 'dp')), may hold values from -0.1875 to 0.1875
Outputs:
- layer_out: bfloat16 [4, 1024, 2048], P('dp', 'sp')
Inputs may be any that keep to these rules, and one draw needn't show every extreme that they name: `routes`: each row names 2 different experts; the rows of one device name one expert at most 16 times, a bound that some block reaches. `forget_cache`: along positions each head's values never rise.
All inputs are finite; a program needn't handle non-finite values.
Results may differ from a plain program's by a relative error of at most 0.0095.
The roundings to bfloat16 on the way count: a program that leaves them out, or rounds other values in their place, can miss the bound.
Values may be sent and summed in bfloat16 or wider, within the bound.
A program may use at most 128 MiB of HBM per device.

v0:
```python
import functools

import jax
import jax.numpy as jnp
from jax import lax
from jax.experimental import pallas as pl
from jax.experimental.pallas import tpu as pltpu
from jax.sharding import PartitionSpec as P

EPS = 1e-06


def norm_rows(inputs, gain):
    floats = inputs.astype(jnp.float32)
    scaled = floats * lax.rsqrt(jnp.mean(floats * floats, axis=-1, keepdims=True) + EPS)
    return (scaled * gain).astype(jnp.bfloat16)


MESH = pl.DeviceIdType.MESH
LANES = 128
BLOCK = 256


def place(index, size):
    return pl.ds(pl.multiple_of(index * size, size), size)


def half_means(squares, head_size):
    lane = lax.broadcasted_iota(jnp.int32, (LANES, LANES), 0) // head_size
    other = lax.broadcasted_iota(jnp.int32, (LANES, LANES), 1) // head_size
    same = (lane == other).astype(jnp.float32).astype(jnp.bfloat16)
    high = squares.astype(jnp.bfloat16)
    low = (squares - high.astype(jnp.float32)).astype(jnp.bfloat16)
    total = jnp.dot(high, same, preferred_element_type=jnp.float32)
    total = total + jnp.dot(low, same, preferred_element_type=jnp.float32)
    return total * (1.0 / head_size)


def attention_kernel(
    n, dp_size, head_size,
    q_ref, k_ref, v_ref, decay_ref, q_gain_ref, k_gain_ref, weight_ref,
    projected_ref, out_ref, weights,
    q_buf, k_buf, v_buf, q_norm, k_head, v_ones, o_buf,
    local_sem, send_sem, recv_sem, own_sem, back_send, back_recv,
    weight_sem, weight_send, weight_recv, pass_send, pass_recv,
):
    me = lax.axis_index("sp")
    column = lax.axis_index("dp")
    rows_y = dp_size // 2
    row_y, core = column // 2, column % 2
    twin = row_y * 2 + 1 - core
    tok = q_ref.shape[0]
    pairs, length = q_buf.shape[0], q_buf.shape[1]
    inner = LANES // head_size
    sources, buffers = (q_ref, k_ref, v_ref), (q_buf, k_buf, v_buf)

    barrier = pltpu.get_barrier_semaphore()
    for step in range(1, n):
        pl.semaphore_signal(
            barrier, inc=1, device_id={"sp": lax.rem(me + step, n)}, device_id_type=MESH
        )
    for step in range(1, rows_y):
        pl.semaphore_signal(
            barrier, inc=1, device_id={"dp": lax.rem(row_y + step, rows_y) * 2 + core},
            device_id_type=MESH,
        )
    pl.semaphore_signal(barrier, inc=1, device_id={"dp": twin}, device_id_type=MESH)
    pl.semaphore_wait(barrier, n - 1 + rows_y)

    def weight_across(step):
        return pltpu.make_async_remote_copy(
            src_ref=weight_ref,
            dst_ref=weights.at[column],
            send_sem=weight_send.at[step],
            recv_sem=weight_recv.at[step],
            device_id={"dp": lax.rem(row_y + step, rows_y) * 2 + core},
            device_id_type=MESH,
        )

    def weight_pass(step):
        block = lax.rem(row_y + rows_y - step, rows_y) * 2 + core
        return pltpu.make_async_remote_copy(
            src_ref=weight_ref if step == 0 else weights.at[block],
            dst_ref=weights.at[block],
            send_sem=pass_send.at[step],
            recv_sem=pass_recv.at[step],
            device_id={"dp": twin},
            device_id_type=MESH,
        )

    weight_own = pltpu.make_async_copy(weight_ref, weights.at[column], weight_sem)

    def outgoing(kind, pair, step):
        target = lax.rem(me + step, n)
        return pltpu.make_async_remote_copy(
            src_ref=sources[kind].at[:, place(target * pairs + pair, LANES)],
            dst_ref=buffers[kind].at[pair, place(me, tok), :],
            send_sem=send_sem.at[kind, pair, step],
            recv_sem=recv_sem.at[kind, pair, step],
            device_id={"sp": target},
            device_id_type=MESH,
        )

    def own(kind, pair):
        return pltpu.make_async_copy(
            sources[kind].at[:, place(me * pairs + pair, LANES)],
            buffers[kind].at[pair, place(me, tok), :],
            local_sem.at[kind, pair],
        )

    def backward(pair, step):
        target = lax.rem(me + step, n)
        return pltpu.make_async_remote_copy(
            src_ref=o_buf.at[pair, place(target, tok), :],
            dst_ref=out_ref.at[:, place(me * pairs + pair, LANES)],
            send_sem=back_send.at[pair, step],
            recv_sem=back_recv.at[pair, step],
            device_id={"sp": target},
            device_id_type=MESH,
        )

    def own_back(pair):
        return pltpu.make_async_copy(
            o_buf.at[pair, place(me, tok), :],
            out_ref.at[:, place(me * pairs + pair, LANES)],
            own_sem.at[pair],
        )

    for pair in range(pairs):
        for step in range(1, n):
            for kind in range(3):
                outgoing(kind, pair, step).start()
        for kind in range(3):
            own(kind, pair).start()

    for step in range(1, rows_y):
        weight_across(step).start()
    weight_pass(0).start()
    weight_own.start()

    row = lax.broadcasted_iota(jnp.int32, (BLOCK, BLOCK), 0)
    col = lax.broadcasted_iota(jnp.int32, (BLOCK, BLOCK), 1)
    lane = lax.broadcasted_iota(jnp.int32, (length, LANES), 1) // head_size
    out_lane = lax.broadcasted_iota(jnp.int32, (BLOCK, LANES), 1) // head_size
    scale = head_size ** (-0.5)
    v_ones[:, LANES:] = jnp.ones((length, LANES), jnp.bfloat16)

    def scores_of(queries, keys):
        return lax.dot_general(
            queries, keys, (((1,), (1,)), ((), ())), preferred_element_type=jnp.float32
        )

    def one_pair(pair, carry):
        for kind in range(3):
            own(kind, pair).wait()
            for step in range(1, n):
                outgoing(kind, pair, step).wait_recv()
        floats = q_buf[pair].astype(jnp.float32)
        floats = floats * lax.rsqrt(half_means(floats * floats, head_size) + EPS)
        normed = (floats * q_gain_ref[...]).astype(jnp.bfloat16)
        q_norm[...] = (normed.astype(jnp.float32) * scale).astype(jnp.bfloat16)
        floats = k_buf[pair].astype(jnp.float32)
        floats = floats * lax.rsqrt(half_means(floats * floats, head_size) + EPS)
        floats = floats * k_gain_ref[...]
        for head in range(inner):
            k_head[head] = jnp.where(lane == head, floats, 0.0).astype(jnp.bfloat16)
        v_ones[:, :LANES] = v_buf[pair]
        for block in range(length // BLOCK):
            first = block * BLOCK
            here = slice(first, first + BLOCK)
            query_block = q_norm[here, :]
            merged = None
            for head in range(inner):
                decay = decay_ref[pl.ds(pair * inner + head, 1), :]
                decay_here = decay[:, here]
                query_decay = jnp.sum(
                    jnp.where(row == col, decay_here, 0.0), axis=1, keepdims=True
                )
                near = scores_of(query_block, k_head[head, here, :])
                near = near + (query_decay - decay_here)
                near = jnp.where(col <= row, near, -jnp.inf)
                highest = jnp.max(near, axis=1, keepdims=True)
                if block > 0:
                    far = scores_of(query_block, k_head[head, :first, :])
                    far = far + (query_decay - decay[:, :first])
                    highest = jnp.maximum(highest, jnp.max(far, axis=1, keepdims=True))
                total = jnp.dot(
                    jnp.exp(near - highest).astype(jnp.bfloat16),
                    v_ones[here, :],
                    preferred_element_type=jnp.float32,
                )
                if block > 0:
                    total = total + jnp.dot(
                        jnp.exp(far - highest).astype(jnp.bfloat16),
                        v_ones[:first, :],
                        preferred_element_type=jnp.float32,
                    )
                result = total[:, :LANES] / total[:, LANES:]
                merged = result if head == 0 else jnp.where(out_lane == head, result, merged)
            o_buf[pair, here, :] = merged.astype(jnp.bfloat16)
        for step in range(1, n):
            backward(pair, step).start()
        own_back(pair).start()
        return carry

    lax.fori_loop(0, pairs, one_pair, 0)
    for step in range(1, rows_y):
        weight_across(step).wait_recv()
        weight_pass(step).start()

    def finish(pair, carry):
        own_back(pair).wait()
        for step in range(1, n):
            backward(pair, step).wait()
            for kind in range(3):
                outgoing(kind, pair, step).wait_send()
        return carry

    lax.fori_loop(0, pairs, finish, 0)
    weight_own.wait()
    for step in range(1, rows_y):
        weight_across(step).wait_send()
    for step in range(rows_y):
        weight_pass(step).wait()
    span = weights.shape[2]
    for block in range(dp_size):
        projected_ref[:, block * span : (block + 1) * span] = jnp.dot(
            out_ref[...], weights[block], preferred_element_type=jnp.float32
        )


def exchange_attention(queries, keys, values, decay, query_gain, key_gain, out_weight):
    tok, width = queries.shape
    n, dp_size = lax.axis_size("sp"), lax.axis_size("dp")
    head_size = query_gain.shape[0]
    inner = LANES // head_size
    pairs = width // n // LANES
    length = n * tok
    return pl.pallas_call(
        functools.partial(attention_kernel, n, dp_size, head_size),
        out_shape=jax.ShapeDtypeStruct((tok, dp_size * out_weight.shape[1]), jnp.float32),
        in_specs=[pl.BlockSpec(memory_space=pltpu.VMEM)] * 6
        + [pl.BlockSpec(memory_space=pl.ANY)],
        out_specs=pl.BlockSpec(memory_space=pltpu.VMEM),
        scratch_shapes=[
            pltpu.VMEM((tok, width), jnp.bfloat16),
            pltpu.VMEM((dp_size,) + out_weight.shape, jnp.bfloat16),
            pltpu.VMEM((pairs, length, LANES), jnp.bfloat16),
            pltpu.VMEM((pairs, length, LANES), jnp.bfloat16),
            pltpu.VMEM((pairs, length, LANES), jnp.bfloat16),
            pltpu.VMEM((length, LANES), jnp.bfloat16),
            pltpu.VMEM((inner, length, LANES), jnp.bfloat16),
            pltpu.VMEM((length, 2 * LANES), jnp.bfloat16),
            pltpu.VMEM((pairs, length, LANES), jnp.bfloat16),
            pltpu.SemaphoreType.DMA((3, pairs)),
            pltpu.SemaphoreType.DMA((3, pairs, n)),
            pltpu.SemaphoreType.DMA((3, pairs, n)),
            pltpu.SemaphoreType.DMA((pairs,)),
            pltpu.SemaphoreType.DMA((pairs, n)),
            pltpu.SemaphoreType.DMA((pairs, n)),
            pltpu.SemaphoreType.DMA,
            pltpu.SemaphoreType.DMA((dp_size,)),
            pltpu.SemaphoreType.DMA((dp_size,)),
            pltpu.SemaphoreType.DMA((dp_size,)),
            pltpu.SemaphoreType.DMA((dp_size,)),
        ],
        compiler_params=pltpu.CompilerParams(
            collective_id=0, has_side_effects=True, vmem_limit_bytes=40 * 1024 * 1024
        ),
        name="attention",
    )(
        queries, keys, values, decay,
        jnp.tile(query_gain, inner)[None, :], jnp.tile(key_gain, inner)[None, :],
        out_weight,
    )


def expert_kernel(
    sp_size, dp_size, per,
    send_ref, gate_ref, up_ref, down_ref,
    out_ref,
    arrived, result, gate_buf, up_buf, down_buf,
    weight_sem, send_sem, recv_sem, back_send, back_recv,
):
    n = sp_size * dp_size
    me = lax.axis_index("sp") * dp_size + lax.axis_index("dp")
    layers = 4 if sp_size % 4 == 0 else 1
    plane = n // layers
    layer, seat = me // plane, me % plane

    def partner(step, sign):
        group, turn = step // plane, step % plane
        high = (layer // 2 + 1 - group // 2) % 2
        low = (layer + (group + 1) // 2) % 2
        other = 2 * high + low if layers == 4 else layer
        return other * plane + (seat + plane + sign * turn) % plane

    cap, width = send_ref.shape[1], send_ref.shape[2]
    loads = [
        pltpu.make_async_copy(source, target, weight_sem.at[index])
        for index, (source, target) in enumerate(
            ((gate_ref, gate_buf), (up_ref, up_buf), (down_ref, down_buf))
        )
    ]
    for load in loads:
        load.start()

    def coords(flat):
        return {"sp": flat // dp_size, "dp": flat % dp_size}

    barrier = pltpu.get_barrier_semaphore()

    def greet(step, carry):
        pl.semaphore_signal(
            barrier, inc=1, device_id=coords((me + step) % n), device_id_type=MESH
        )
        return carry

    lax.fori_loop(1, n, greet, 0)
    pl.semaphore_wait(barrier, n - 1)

    def outgoing(step):
        target = partner(step, 1)
        return pltpu.make_async_remote_copy(
            src_ref=send_ref.at[target],
            dst_ref=arrived.at[step],
            send_sem=send_sem.at[step],
            recv_sem=recv_sem.at[step],
            device_id=coords(target),
            device_id_type=MESH,
        )

    def backward(step):
        target = partner(step, -1)
        return pltpu.make_async_remote_copy(
            src_ref=result.at[step],
            dst_ref=out_ref.at[me],
            send_sem=back_send.at[step],
            recv_sem=back_recv.at[step],
            device_id=coords(target),
            device_id_type=MESH,
        )

    mine = n - plane
    own = pltpu.make_async_copy(send_ref.at[me], arrived.at[mine], recv_sem.at[mine])
    own_back = pltpu.make_async_copy(result.at[mine], out_ref.at[me], back_recv.at[mine])

    def launch(step, carry):
        outgoing(step).start()
        return carry

    lax.fori_loop(0, mine, launch, 0)
    lax.fori_loop(mine + 1, n, launch, 0)
    own.start()
    for load in loads:
        load.wait()

    def chunk(index, carry):
        first = index * per
        for offset in range(per):
            if offset == 0:
                @pl.when(first == mine)
                def _():
                    own.wait()

                @pl.when(first != mine)
                def _():
                    outgoing(first).wait_recv()
            else:
                outgoing(first + offset).wait_recv()
        rows = arrived[pl.ds(first, per)].reshape(per * cap, width)
        gate = jnp.dot(rows, gate_buf[...], preferred_element_type=jnp.float32)
        upper = jnp.dot(rows, up_buf[...], preferred_element_type=jnp.float32)
        hidden = (gate / (1.0 + jnp.exp(-gate)) * upper).astype(jnp.bfloat16)
        product = jnp.dot(hidden, down_buf[...], preferred_element_type=jnp.float32)
        result[pl.ds(first, per)] = product.astype(jnp.bfloat16).reshape(per, cap, width)
        for offset in range(per):
            if offset == 0:
                @pl.when(first == mine)
                def _():
                    own_back.start()

                @pl.when(first != mine)
                def _():
                    backward(first).start()
            else:
                backward(first + offset).start()
        return carry

    lax.fori_loop(0, n // per, chunk, 0)

    def finish(step, carry):
        outgoing(step).wait_send()
        backward(step).wait()
        return carry

    own_back.wait()
    lax.fori_loop(0, mine, finish, 0)
    lax.fori_loop(mine + 1, n, finish, 0)


def run_experts(send, gate, upper, down):
    n, cap, width = send.shape
    sp_size, dp_size = lax.axis_size("sp"), lax.axis_size("dp")
    per = max(1, min(n, LANES // cap))
    return pl.pallas_call(
        functools.partial(expert_kernel, sp_size, dp_size, per),
        out_shape=jax.ShapeDtypeStruct(send.shape, jnp.bfloat16),
        in_specs=[pl.BlockSpec(memory_space=pltpu.VMEM)]
        + [pl.BlockSpec(memory_space=pl.ANY)] * 3,
        out_specs=pl.BlockSpec(memory_space=pltpu.VMEM),
        scratch_shapes=[
            pltpu.VMEM(send.shape, jnp.bfloat16),
            pltpu.VMEM(send.shape, jnp.bfloat16),
            pltpu.VMEM(gate.shape, jnp.bfloat16),
            pltpu.VMEM(upper.shape, jnp.bfloat16),
            pltpu.VMEM(down.shape, jnp.bfloat16),
            pltpu.SemaphoreType.DMA((3,)),
            pltpu.SemaphoreType.DMA((n,)),
            pltpu.SemaphoreType.DMA((n,)),
            pltpu.SemaphoreType.DMA((n,)),
            pltpu.SemaphoreType.DMA((n,)),
        ],
        compiler_params=pltpu.CompilerParams(
            collective_id=1, has_side_effects=True, vmem_limit_bytes=56 * 1024 * 1024
        ),
        name="experts",
    )(send, gate, upper, down)


def shards(
    resid,
    queries,
    keys,
    values,
    forget_cache,
    query_gain,
    key_gain,
    out_weight,
    norm_gain,
    routes,
    group_weight,
    inner_share,
    expert_gate,
    expert_up,
    expert_down,
):
    projected = exchange_attention(
        queries[0], keys[0], values[0], forget_cache[0], query_gain, key_gain, out_weight
    )
    mid = (resid[0].astype(jnp.float32) + projected).astype(jnp.bfloat16)
    normed = norm_rows(mid, norm_gain)
    width = normed.shape[1]
    tok_count = normed.shape[0]
    top_count = routes.shape[2]
    experts = lax.axis_size("sp") * lax.axis_size("dp")
    capacity = 2 * tok_count * top_count // experts
    expert_ids = routes[0].reshape(-1)
    expert_onehot = (expert_ids[:, None] == jnp.arange(experts, dtype=jnp.int32)[None, :]).astype(
        jnp.int32
    )
    earlier = jnp.cumsum(expert_onehot, axis=0) - expert_onehot
    slot_rank = jnp.sum(earlier * expert_onehot, axis=1)
    slot_index = (expert_ids * capacity + slot_rank).reshape(tok_count, top_count)
    slot_range = jnp.arange(experts * capacity, dtype=jnp.int32)
    dispatch = jnp.any(slot_range[:, None, None] == slot_index[None, :, :], axis=2).astype(
        jnp.bfloat16
    )
    send = jnp.dot(dispatch, normed, preferred_element_type=jnp.float32).astype(jnp.bfloat16)
    returned = run_experts(
        send.reshape(experts, capacity, width), expert_gate[0], expert_up[0], expert_down[0]
    )
    returned = returned.reshape(experts * capacity, width)
    shares = inner_share[0]
    weights = group_weight[0][:, None] * shares / jnp.sum(shares, axis=-1, keepdims=True)
    mixed = jnp.zeros((tok_count, width), jnp.float32)
    for route in range(top_count):
        select = (slot_range[None, :] == slot_index[:, route : route + 1]).astype(jnp.bfloat16)
        picked = jnp.dot(select, returned, preferred_element_type=jnp.float32)
        mixed = mixed + weights[:, route : route + 1] * picked
    layer_out = (mid.astype(jnp.float32) + mixed).astype(jnp.bfloat16)
    return layer_out.reshape(1, tok_count, width)


def solution(mesh):
    return jax.shard_map(
        shards,
        mesh=mesh,
        in_specs=(
            P("dp", "sp", None),
            P("dp", "sp", None),
            P("dp", "sp", None),
            P("dp", "sp", None),
            P("dp", "sp", None),
            P(),
            P(),
            P(None, "dp"),
            P(),
            P("dp", "sp", None),
            P("dp", "sp"),
            P("dp", "sp", None),
            P(("sp", "dp"), None, None),
            P(("sp", "dp"), None, None),
            P(("sp", "dp"), None, None),
        ),
        out_specs=P("dp", "sp", None),
        check_vma=False,
    )
```

profile of v0, /device:TPU:0, one launch (start us, length us, event | category | flops | bytes accessed | tf_op | source)
XLA Modules:
  0.0 176.9 jit_solution(1797798232868527673)
XLA Ops:
  0.0 0.7 reduce_sum.31
  0.7 0.7 fusion.18
  1.4 0.7 tile.4
  2.0 0.1 broadcast_in_dim_tile.6.q_gain_ref
  2.1 0.7 tile.5
  2.8 0.1 broadcast_in_dim_tile.7.k_gain_ref
  2.9 0.8 copy.25
  3.7 0.1 eq.75
  3.8 0.1 eq.71
  4.0 0.6 reduce-window.6
  4.5 0.2 slice_reduce_fusion.2
  4.8 0.1 fusion.16
  4.9 0.1 reduce_sum.34
  5.0 0.1 copy.29
  5.1 0.1 fusion.11
  5.2 0.1 reduce_sum.33
  5.4 0.2 slice_reduce_fusion
  5.5 0.0 copy-start
  5.5 1.6 copy-done
  7.1 0.0 copy-start.1
  7.1 1.0 copy-done.1
  8.2 0.0 copy-start.2
  8.2 1.0 copy-done.2
  9.2 0.0 copy-start.3
  9.2 1.0 copy-done.3
  10.3 0.0 copy-start.4
  10.3 0.7 copy-done.4
  11.0 0.0 copy-start.6
  11.0 59.5 %attention.1 = f32[128,2048]{1,0:T(8,128)S(1)} custom-call(bf16[128,2048]{1,0:T(8,128)(2,1)S(1)} %bitcast.50, bf16[128,2048]{1,0:T(8,128)(2,1)S(1)} %bitcast.51, bf16[128,2048]{1,0:T(8,128)(2,1)S(1)} %bitcast.52, f32[4,1024]{1,0:T(4,128)S(1)} %bitcast.53, f32[1,128]{1,0:T(1,128)S(1)} %broadcast_in_dim_tile.6.q_gain_ref, ...), custom_call_target="tpu_custom_call" | custom-call | tf_op jit(solution)/shard_map/attention/pallas_call | solution.py:239
  70.5 0.0 copy-done.6
  70.5 0.0 copy-start.7
  70.5 0.3 fusion.4
  70.8 0.4 copy-done.7
  71.2 2.1 %convolution_convert_fusion = bf16[512,2048]{1,0:T(8,128)(2,1)} fusion(pred[512,128]{1,0:T(8,128)(4,1)S(1)} %fusion.11, bf16[128,2048]{1,0:T(8,128)(2,1)S(1)} %get-tuple-element.8, f32[2048]{0:T(1024)S(1)} %copy-done.7, f32[128]{0:T(128)S(1)} %add_rsqrt_fusion), kind=kOutput, calls=%fused_computation | convolution fusion | flops 270532608 | bytes 2695680 | tf_op jit(solution)/shard_map/dot_general | solution.py:469
  73.4 99.9 %experts.1 = bf16[32,16,2048]{2,1,0:T(8,128)(2,1)} custom-call(bf16[32,16,2048]{2,1,0:T(8,128)(2,1)} %bitcast.56, bf16[2048,1024]{1,0:T(8,128)(2,1)} %bitcast.57, bf16[2048,1024]{1,0:T(8,128)(2,1)} %bitcast.58, bf16[1024,2048]{1,0:T(8,128)(2,1)} %bitcast.59), custom_call_target="tpu_custom_call" | custom-call | tf_op jit(solution)/shard_map/experts/pallas_call | solution.py:406
  173.3 0.0 copy-start.5
  173.3 2.2 %convolution_multiply_fusion.1 = f32[128,2048]{1,0:T(8,128)S(1)} fusion(bf16[512,2048]{1,0:T(8,128)(2,1)} %bitcast.54, f32[128]{0:T(128)S(1)} %get-tuple-element.10, s32[128]{0:T(128)S(1)} %get-tuple-element.6), kind=kOutput, calls=%fused_computation.4 | convolution fusion | flops 268763136 | bytes 3146752 | tf_op jit(solution)/shard_map/dot_general | solution.py:479
  175.5 0.0 copy-done.5
  175.5 1.4 fusion.3
  (7 shorter events, 0.1 us)
Async XLA Ops:
  5.5 1.6 copy-start
  7.1 1.0 copy-start.1
  8.2 1.0 copy-start.2
  9.2 1.0 copy-start.3
  10.3 0.7 copy-start.4
  11.0 59.5 %copy-start.6 = (bf16[1,128,2048]{2,1,0:T(8,128)(2,1)S(1)}, bf16[1,128,2048]{2,1,0:T(8,128)(2,1)}, u32[]{:S(2)}) copy-start(bf16[1,128,2048]{2,1,0:T(8,128)(2,1)} %param.15) | copy-start | bytes 1572868
  70.5 0.7 copy-start.7
  173.3 2.2 %copy-start.5 = (bf16[32,16,2048]{2,1,0:T(8,128)(2,1)S(1)}, bf16[32,16,2048]{2,1,0:T(8,128)(2,1)}, u32[]{:S(2)}) copy-start(bf16[32,16,2048]{2,1,0:T(8,128)(2,1)} %experts.1) | copy-start | bytes 6291460
where the time goes:
time: 177 us
  Pallas kernels  159 us (90%)
  local copies, waits for them, and re-layouts  9.12 us (5%)
  matrix products  5.71 us (3%)
  other arithmetic  2.48 us (1%)
    pallas_call x1, Pallas kernels, run_experts(): pl.pallas_call(functools.partial(expert_kernel, sp_size, dp_size, per), o...  99.9 us
    pallas_call x1, Pallas kernels, exchange_attention(): pl.pallas_call(functools.partial(attention_kernel, n, dp_size, head_size)...  59.5 us
    unnamed x17, local copies, waits for them, and re-layouts  6.65 us
    dot_general x2, matrix products, shards(): picked = jnp.dot(select, returned, preferred_element_type=jnp.float32)  3.58 us

commit v1 on v0

v1 whole, which is shorter than its diff:
```python
import functools

import jax
import jax.numpy as jnp
from jax import lax
from jax.experimental import pallas as pl
from jax.experimental.pallas import tpu as pltpu
from jax.sharding import PartitionSpec as P

EPS = 1e-06


MESH = pl.DeviceIdType.MESH
LANES = 128
BLOCK = 256


def place(index, size):
    return pl.ds(pl.multiple_of(index * size, size), size)


def half_means(squares, head_size):
    lane = lax.broadcasted_iota(jnp.int32, (LANES, LANES), 0) // head_size
    other = lax.broadcasted_iota(jnp.int32, (LANES, LANES), 1) // head_size
    same = (lane == other).astype(jnp.float32).astype(jnp.bfloat16)
    high = squares.astype(jnp.bfloat16)
    low = (squares - high.astype(jnp.float32)).astype(jnp.bfloat16)
    total = jnp.dot(high, same, preferred_element_type=jnp.float32)
    total = total + jnp.dot(low, same, preferred_element_type=jnp.float32)
    return total * (1.0 / head_size)


def attention_stage(
    n, dp_size, head_size, small_loads, weight_loads,
    q_ref, k_ref, v_ref, weight_ref, resid_ref,
    decay_ref, q_gain_ref, k_gain_ref, norm_gain_ref, routes_ref, group_ref, share_ref,
    mid_ref, normed_ref, info_ref, out_ref, weights, resid_buf,
    q_buf, k_buf, v_buf, q_norm, k_head, v_ones, o_buf,
    local_sem, send_sem, recv_sem, own_sem, back_send, back_recv,
    weight_sem, weight_send, weight_recv, pass_send, pass_recv, resid_sem,
):
    me = lax.axis_index("sp")
    column = lax.axis_index("dp")
    rows_y = dp_size // 2
    row_y, core = column // 2, column % 2
    twin = row_y * 2 + 1 - core
    tok = q_ref.shape[0]
    pairs, length = q_buf.shape[0], q_buf.shape[1]
    inner = LANES // head_size
    sources, buffers = (q_ref, k_ref, v_ref), (q_buf, k_buf, v_buf)

    def weight_across(step):
        return pltpu.make_async_remote_copy(
            src_ref=weight_ref,
            dst_ref=weights.at[column],
            send_sem=weight_send.at[step],
            recv_sem=weight_recv.at[step],
            device_id={"dp": lax.rem(row_y + step, rows_y) * 2 + core},
            device_id_type=MESH,
        )

    def weight_pass(step):
        block = lax.rem(row_y + rows_y - step, rows_y) * 2 + core
        return pltpu.make_async_remote_copy(
            src_ref=weight_ref if step == 0 else weights.at[block],
            dst_ref=weights.at[block],
            send_sem=pass_send.at[step],
            recv_sem=pass_recv.at[step],
            device_id={"dp": twin},
            device_id_type=MESH,
        )

    weight_own = pltpu.make_async_copy(weight_ref, weights.at[column], weight_sem)

    def outgoing(kind, pair, step):
        target = lax.rem(me + step, n)
        return pltpu.make_async_remote_copy(
            src_ref=sources[kind].at[:, place(target * pairs + pair, LANES)],
            dst_ref=buffers[kind].at[pair, place(me, tok), :],
            send_sem=send_sem.at[kind, pair, step],
            recv_sem=recv_sem.at[kind, pair, step],
            device_id={"sp": target},
            device_id_type=MESH,
        )

    def own(kind, pair):
        return pltpu.make_async_copy(
            sources[kind].at[:, place(me * pairs + pair, LANES)],
            buffers[kind].at[pair, place(me, tok), :],
            local_sem.at[kind, pair],
        )

    def backward(pair, step):
        target = lax.rem(me + step, n)
        return pltpu.make_async_remote_copy(
            src_ref=o_buf.at[pair, place(target, tok), :],
            dst_ref=out_ref.at[:, place(me * pairs + pair, LANES)],
            send_sem=back_send.at[pair, step],
            recv_sem=back_recv.at[pair, step],
            device_id={"sp": target},
            device_id_type=MESH,
        )

    def own_back(pair):
        return pltpu.make_async_copy(
            o_buf.at[pair, place(me, tok), :],
            out_ref.at[:, place(me * pairs + pair, LANES)],
            own_sem.at[pair],
        )

    for pair in range(pairs):
        for step in range(1, n):
            for kind in range(3):
                outgoing(kind, pair, step).start()
        for kind in range(3):
            own(kind, pair).start()

    for step in range(1, rows_y):
        weight_across(step).start()
    weight_pass(0).start()
    weight_own.start()
    load_resid = pltpu.make_async_copy(resid_ref, resid_buf, resid_sem)
    load_resid.start()
    for load in weight_loads:
        load.start()
    for load in small_loads:
        load.wait()
    info_ref[...] = routing_info(routes_ref, group_ref, share_ref, n * dp_size)
    q_gain = jnp.concatenate([q_gain_ref[...]] * inner, axis=1)
    k_gain = jnp.concatenate([k_gain_ref[...]] * inner, axis=1)

    row = lax.broadcasted_iota(jnp.int32, (BLOCK, BLOCK), 0)
    col = lax.broadcasted_iota(jnp.int32, (BLOCK, BLOCK), 1)
    lane = lax.broadcasted_iota(jnp.int32, (length, LANES), 1) // head_size
    out_lane = lax.broadcasted_iota(jnp.int32, (BLOCK, LANES), 1) // head_size
    scale = head_size ** (-0.5)
    v_ones[:, LANES:] = jnp.ones((length, LANES), jnp.bfloat16)

    def scores_of(queries, keys):
        return lax.dot_general(
            queries, keys, (((1,), (1,)), ((), ())), preferred_element_type=jnp.float32
        )

    def one_pair(pair, carry):
        for kind in range(3):
            own(kind, pair).wait()
            for step in range(1, n):
                outgoing(kind, pair, step).wait_recv()
        floats = q_buf[pair].astype(jnp.float32)
        floats = floats * lax.rsqrt(half_means(floats * floats, head_size) + EPS)
        normed = (floats * q_gain).astype(jnp.bfloat16)
        q_norm[...] = (normed.astype(jnp.float32) * scale).astype(jnp.bfloat16)
        floats = k_buf[pair].astype(jnp.float32)
        floats = floats * lax.rsqrt(half_means(floats * floats, head_size) + EPS)
        floats = floats * k_gain
        for head in range(inner):
            k_head[head] = jnp.where(lane == head, floats, 0.0).astype(jnp.bfloat16)
        v_ones[:, :LANES] = v_buf[pair]
        for block in range(length // BLOCK):
            first = block * BLOCK
            here = slice(first, first + BLOCK)
            query_block = q_norm[here, :]
            merged = None
            for head in range(inner):
                decay = decay_ref[pl.ds(pair * inner + head, 1), :]
                decay_here = decay[:, here]
                query_decay = jnp.sum(
                    jnp.where(row == col, decay_here, 0.0), axis=1, keepdims=True
                )
                near = scores_of(query_block, k_head[head, here, :])
                near = near + (query_decay - decay_here)
                near = jnp.where(col <= row, near, -jnp.inf)
                highest = jnp.max(near, axis=1, keepdims=True)
                if block > 0:
                    far = scores_of(query_block, k_head[head, :first, :])
                    far = far + (query_decay - decay[:, :first])
                    highest = jnp.maximum(highest, jnp.max(far, axis=1, keepdims=True))
                total = jnp.dot(
                    jnp.exp(near - highest).astype(jnp.bfloat16),
                    v_ones[here, :],
                    preferred_element_type=jnp.float32,
                )
                if block > 0:
                    total = total + jnp.dot(
                        jnp.exp(far - highest).astype(jnp.bfloat16),
                        v_ones[:first, :],
                        preferred_element_type=jnp.float32,
                    )
                result = total[:, :LANES] / total[:, LANES:]
                merged = result if head == 0 else jnp.where(out_lane == head, result, merged)
            o_buf[pair, here, :] = merged.astype(jnp.bfloat16)
        for step in range(1, n):
            backward(pair, step).start()
        own_back(pair).start()
        return carry

    lax.fori_loop(0, pairs, one_pair, 0)
    for step in range(1, rows_y):
        weight_across(step).wait_recv()
        weight_pass(step).start()

    def finish(pair, carry):
        own_back(pair).wait()
        for step in range(1, n):
            backward(pair, step).wait()
            for kind in range(3):
                outgoing(kind, pair, step).wait_send()
        return carry

    lax.fori_loop(0, pairs, finish, 0)
    weight_own.wait()
    for step in range(1, rows_y):
        weight_across(step).wait_send()
    for step in range(rows_y):
        weight_pass(step).wait()
    load_resid.wait()
    span = weights.shape[2]
    squares = jnp.zeros((tok, 1), jnp.float32)
    for block in range(dp_size):
        columns = slice(block * span, (block + 1) * span)
        projected = jnp.dot(
            out_ref[...], weights[block], preferred_element_type=jnp.float32
        )
        mid = (resid_buf[:, columns].astype(jnp.float32) + projected).astype(jnp.bfloat16)
        mid_ref[:, columns] = mid
        floats = mid.astype(jnp.float32)
        squares = squares + jnp.sum(floats * floats, axis=1, keepdims=True)
    factor = lax.rsqrt(squares * (1.0 / (dp_size * span)) + EPS)
    for block in range(dp_size):
        columns = slice(block * span, (block + 1) * span)
        scaled = mid_ref[:, columns].astype(jnp.float32) * factor
        normed_ref[:, columns] = (scaled * norm_gain_ref[:, columns]).astype(jnp.bfloat16)


INFO_ROWS = 8


def routing_info(routes_ref, group_ref, share_ref, experts):
    top, tok = routes_ref.shape
    capacity = 2 * tok * top // experts
    expert = lax.broadcasted_iota(jnp.int32, (experts, tok), 0)
    hits = [(expert == routes_ref[r : r + 1, :]).astype(jnp.float32) for r in range(top)]
    every = sum(hits[1:], hits[0]).astype(jnp.bfloat16)
    row = lax.broadcasted_iota(jnp.int32, (tok, tok), 0)
    col = lax.broadcasted_iota(jnp.int32, (tok, tok), 1)
    before = (row < col).astype(jnp.float32).astype(jnp.bfloat16)
    earlier = jnp.dot(every, before, preferred_element_type=jnp.float32)
    shares = [share_ref[r : r + 1, :] for r in range(top)]
    total = sum(shares[1:], shares[0])
    lines = [
        routes_ref[r : r + 1, :].astype(jnp.float32) * capacity
        + jnp.sum(hits[r] * earlier, axis=0, keepdims=True)
        for r in range(top)
    ]
    lines += [group_ref[...] * shares[r] / total for r in range(top)]
    lines.append(jnp.zeros((INFO_ROWS - 2 * top, tok), jnp.float32))
    return jnp.concatenate(lines, axis=0)


CHUNKS = 4


def expert_stage(
    sp_size, dp_size, per, top, weight_loads,
    mid_ref, normed_ref, info_ref, gate_buf, up_buf, down_buf,
    out_ref,
    far_rows, far_info, packed, arrived, result, returned, partial, incoming,
    info_sem, row_send, row_recv, send_sem, recv_sem,
    back_send, back_recv, sum_send, sum_recv,
):
    n = sp_size * dp_size
    half = n // 2
    me = lax.axis_index("sp") * dp_size + lax.axis_index("dp")
    side, seat = me // half, me % half
    twin = (me + half) % n
    tok, width = normed_ref.shape
    cap = packed.shape[2]
    part = width // CHUNKS
    mine = half // 2

    def columns(chunk):
        return slice(chunk * part, (chunk + 1) * part)

    def coords(flat):
        return {"sp": flat // dp_size, "dp": flat % dp_size}

    info_copy = pltpu.make_async_remote_copy(
        src_ref=info_ref, dst_ref=far_info, send_sem=info_sem.at[0], recv_sem=info_sem.at[1],
        device_id=coords(twin), device_id_type=MESH,
    )
    row_copies = [
        pltpu.make_async_remote_copy(
            src_ref=normed_ref.at[:, columns(chunk)],
            dst_ref=far_rows.at[:, columns(chunk)],
            send_sem=row_send.at[chunk],
            recv_sem=row_recv.at[chunk],
            device_id=coords(twin),
            device_id_type=MESH,
        )
        for chunk in range(CHUNKS)
    ]

    def outgoing(kind, step, chunk):
        target = (seat + mine + step) % half
        return pltpu.make_async_remote_copy(
            src_ref=packed.at[kind, target, :, columns(chunk)],
            dst_ref=arrived.at[kind, step, :, columns(chunk)],
            send_sem=send_sem.at[kind, chunk, step],
            recv_sem=recv_sem.at[kind, chunk, step],
            device_id=coords(side * half + target),
            device_id_type=MESH,
        )

    def backward(kind, step, chunk):
        target = (seat + half + half - mine - step) % half
        return pltpu.make_async_remote_copy(
            src_ref=result.at[kind, step, :, columns(chunk)],
            dst_ref=returned.at[kind, seat, :, columns(chunk)],
            send_sem=back_send.at[kind, chunk, step],
            recv_sem=back_recv.at[kind, chunk, step],
            device_id=coords(side * half + target),
            device_id_type=MESH,
        )

    def sum_copy(chunk):
        return pltpu.make_async_remote_copy(
            src_ref=partial.at[chunk],
            dst_ref=incoming.at[chunk],
            send_sem=sum_send.at[chunk],
            recv_sem=sum_recv.at[chunk],
            device_id=coords(twin),
            device_id_type=MESH,
        )

    def others(action, start=0, stop=half):
        def run(step, carry):
            @pl.when(step != mine)
            def _():
                action(step)

            return carry

        lax.fori_loop(start, stop, run, 0)

    first_slot = (side * (half * cap)).astype(jnp.float32)

    def dispatch(kind, source_ref, route_ref, chunk):
        slot = lax.broadcasted_iota(jnp.int32, (half * cap, tok), 0).astype(jnp.float32)
        hit = jnp.zeros((half * cap, tok), jnp.float32)
        for route in range(top):
            local = route_ref[route : route + 1, :] - first_slot
            hit = hit + jnp.where(slot == local, 1.0, 0.0)
        rows = jnp.dot(
            hit.astype(jnp.bfloat16), source_ref[:, columns(chunk)],
            preferred_element_type=jnp.float32,
        )
        packed[kind, :, :, columns(chunk)] = rows.astype(jnp.bfloat16).reshape(half, cap, part)
        others(lambda step: outgoing(kind, step, chunk).start())
        arrived[kind, mine, :, columns(chunk)] = packed[kind, seat, :, columns(chunk)]

    def forward(kind, send_back):
        def group(index, carry):
            first = index * per

            def take(step):
                for chunk in range(CHUNKS):
                    outgoing(kind, step, chunk).wait_recv()

            others(take, first, first + per)
            rows = arrived[kind, pl.ds(first, per)].reshape(per * cap, width)
            gate = jnp.dot(rows, gate_buf[...], preferred_element_type=jnp.float32)
            upper = jnp.dot(rows, up_buf[...], preferred_element_type=jnp.float32)
            hidden = (gate / (1.0 + jnp.exp(-gate)) * upper).astype(jnp.bfloat16)
            for chunk in range(CHUNKS):
                product = jnp.dot(
                    hidden, down_buf[:, columns(chunk)], preferred_element_type=jnp.float32
                )
                result[kind, pl.ds(first, per), :, columns(chunk)] = product.astype(
                    jnp.bfloat16
                ).reshape(per, cap, part)
                if send_back:
                    others(lambda step: backward(kind, step, chunk).start(), first, first + per)
            return carry

        lax.fori_loop(0, half // per, group, 0)
        returned[kind, seat] = result[kind, mine]

    row = lax.broadcasted_iota(jnp.int32, (tok, tok), 0)
    col = lax.broadcasted_iota(jnp.int32, (tok, tok), 1)

    def upright(line):
        return jnp.sum(jnp.where(row == col, line, 0.0), axis=1, keepdims=True)

    def choices(route_ref):
        slot = lax.broadcasted_iota(jnp.int32, (tok, half * cap), 1).astype(jnp.float32)
        picks = []
        for route in range(top):
            local = upright(route_ref[route : route + 1, :]) - first_slot
            pick = jnp.where(slot == local, 1.0, 0.0).astype(jnp.bfloat16)
            picks.append((pick, upright(route_ref[top + route : top + route + 1, :])))
        return picks

    def combine(kind, picks, chunk):
        others(lambda step: backward(kind, step, chunk).wait_recv())
        block = returned[kind, :, :, columns(chunk)].reshape(half * cap, part)
        total = None
        for pick, weight in picks:
            term = weight * jnp.dot(pick, block, preferred_element_type=jnp.float32)
            total = term if total is None else total + term
        return total

    info_copy.start()
    for copy in row_copies:
        copy.start()
    for chunk in range(CHUNKS):
        dispatch(0, normed_ref, info_ref, chunk)
    info_copy.wait_recv()
    for chunk in range(CHUNKS):
        row_copies[chunk].wait_recv()
        dispatch(1, far_rows, far_info, chunk)
    for load in weight_loads:
        load.wait()
    forward(0, False)
    forward(1, True)
    for chunk in range(CHUNKS):
        others(lambda step: backward(0, step, chunk).start())
    far_picks = choices(far_info)
    for chunk in range(CHUNKS):
        partial[chunk] = combine(1, far_picks, chunk).astype(jnp.bfloat16)
        sum_copy(chunk).start()
    picks = choices(info_ref)
    for chunk in range(CHUNKS):
        total = combine(0, picks, chunk)
        sum_copy(chunk).wait_recv()
        total = total + incoming[chunk].astype(jnp.float32)
        out_ref[:, columns(chunk)] = mid_ref[:, columns(chunk)].astype(jnp.float32) + total

    info_copy.wait_send()
    for chunk in range(CHUNKS):
        row_copies[chunk].wait_send()
        sum_copy(chunk).wait_send()

    def drain(step):
        for kind in range(2):
            for chunk in range(CHUNKS):
                outgoing(kind, step, chunk).wait_send()
                backward(kind, step, chunk).wait_send()

    others(drain)


def layer_kernel(sp_size, dp_size, head_size, per, top, *refs):
    inputs, out_ref, scratch = refs[:15], refs[15], refs[16:]
    (
        q_ref, k_ref, v_ref, weight_ref, resid_ref, gate_ref, up_ref, down_ref,
    ) = inputs[:8]
    small = scratch[:7]
    gate_buf, up_buf, down_buf, mid_ref, normed_ref, info_ref = scratch[7:13]
    small_sem, load_sem = scratch[13:15]
    attention_scratch, expert_scratch = scratch[15:37], scratch[37:]
    small_loads = [
        pltpu.make_async_copy(source, target, small_sem.at[index])
        for index, (source, target) in enumerate(zip(inputs[8:], small))
    ]
    weight_loads = [
        pltpu.make_async_copy(source, target, load_sem.at[index])
        for index, (source, target) in enumerate(
            ((gate_ref, gate_buf), (up_ref, up_buf), (down_ref, down_buf))
        )
    ]
    for load in small_loads:
        load.start()
    n = sp_size * dp_size
    me = lax.axis_index("sp") * dp_size + lax.axis_index("dp")
    barrier = pltpu.get_barrier_semaphore()

    def greet(step, carry):
        other = (me + step) % n
        pl.semaphore_signal(
            barrier, inc=1, device_id={"sp": other // dp_size, "dp": other % dp_size},
            device_id_type=MESH,
        )
        return carry

    lax.fori_loop(1, n, greet, 0)
    pl.semaphore_wait(barrier, n - 1)
    attention_stage(
        sp_size, dp_size, head_size, small_loads, weight_loads,
        q_ref, k_ref, v_ref, weight_ref, resid_ref, *small,
        mid_ref, normed_ref, info_ref, *attention_scratch,
    )
    expert_stage(
        sp_size, dp_size, per, top, weight_loads,
        mid_ref, normed_ref, info_ref, gate_buf, up_buf, down_buf, out_ref, *expert_scratch,
    )


def run_layer(
    queries, keys, values, out_weight, resid, gate, upper, down,
    decay, query_gain, key_gain, norm_gain, routes, group_weight, inner_share,
):
    tok, width = queries.shape
    sp_size, dp_size = lax.axis_size("sp"), lax.axis_size("dp")
    top = routes.shape[0]
    head_size = query_gain.shape[1]
    inner = LANES // head_size
    pairs = width // sp_size // LANES
    length = sp_size * tok
    n = sp_size * dp_size
    half = n // 2
    cap = 2 * tok * top // n
    per = max(1, min(half, LANES // cap))
    small = (decay, query_gain, key_gain, norm_gain, routes, group_weight, inner_share)
    dma = pltpu.SemaphoreType.DMA
    rows = pltpu.VMEM((tok, width), jnp.bfloat16)
    info = pltpu.VMEM((INFO_ROWS, tok), jnp.float32)
    head_pairs = pltpu.VMEM((pairs, length, LANES), jnp.bfloat16)
    blocks = pltpu.VMEM((2, half, cap, width), jnp.bfloat16)
    sums = pltpu.VMEM((CHUNKS, tok, width // CHUNKS), jnp.bfloat16)
    flags = dma((2, CHUNKS, half))
    chunk_flags = dma((CHUNKS,))
    scratch = [pltpu.VMEM(array.shape, array.dtype) for array in small]
    scratch += [pltpu.VMEM(array.shape, array.dtype) for array in (gate, upper, down)]
    scratch += [rows, rows, info, dma((len(small),)), dma((3,))]
    attention_scratch = [
        rows,
        pltpu.VMEM((dp_size,) + out_weight.shape, jnp.bfloat16),
        rows,
        head_pairs,
        head_pairs,
        head_pairs,
        pltpu.VMEM((length, LANES), jnp.bfloat16),
        pltpu.VMEM((inner, length, LANES), jnp.bfloat16),
        pltpu.VMEM((length, 2 * LANES), jnp.bfloat16),
        head_pairs,
        dma((3, pairs)),
        dma((3, pairs, sp_size)),
        dma((3, pairs, sp_size)),
        dma((pairs,)),
        dma((pairs, sp_size)),
        dma((pairs, sp_size)),
        dma,
        dma((dp_size,)),
        dma((dp_size,)),
        dma((dp_size,)),
        dma((dp_size,)),
        dma,
    ]
    expert_scratch = [
        rows, info, blocks, blocks, blocks, blocks, sums, sums,
        dma((2,)), chunk_flags, chunk_flags,
        flags, flags, flags, flags,
        chunk_flags, chunk_flags,
    ]
    in_hbm = pl.BlockSpec(memory_space=pltpu.HBM)
    return pl.pallas_call(
        functools.partial(layer_kernel, sp_size, dp_size, head_size, per, top),
        out_shape=jax.ShapeDtypeStruct((tok, width), jnp.float32),
        in_specs=[in_hbm] * 15,
        out_specs=pl.BlockSpec(memory_space=pltpu.VMEM),
        scratch_shapes=scratch + attention_scratch + expert_scratch,
        compiler_params=pltpu.CompilerParams(
            collective_id=0, has_side_effects=True, vmem_limit_bytes=VMEM_LIMIT
        ),
        name="layer",
    )(queries, keys, values, out_weight, resid, gate, upper, down, *small)


VMEM_LIMIT = 62 * 1024 * 1024


def shards(
    resid,
    queries,
    keys,
    values,
    forget_cache,
    query_gain,
    key_gain,
    out_weight,
    norm_gain,
    routes,
    group_weight,
    inner_share,
    expert_gate,
    expert_up,
    expert_down,
):
    total = run_layer(
        queries[0], keys[0], values[0], out_weight, resid[0],
        expert_gate[0], expert_up[0], expert_down[0],
        forget_cache[0], query_gain[None], key_gain[None], norm_gain[None],
        routes[0].T, group_weight, inner_share[0].T,
    )
    return total.astype(jnp.bfloat16)[None]


def solution(mesh):
    return jax.shard_map(
        shards,
        mesh=mesh,
        in_specs=(
            P("dp", "sp", None),
            P("dp", "sp", None),
            P("dp", "sp", None),
            P("dp", "sp", None),
            P("dp", "sp", None),
            P(),
            P(),
            P(None, "dp"),
            P(),
            P("dp", "sp", None),
            P("dp", "sp"),
            P("dp", "sp", None),
            P(("sp", "dp"), None, None),
            P(("sp", "dp"), None, None),
            P(("sp", "dp"), None, None),
        ),
        out_specs=P("dp", "sp", None),
        check_vma=False,
    )
```

time: 177 us -> 144 us (0.81)
  Pallas kernels: 159 us -> 142 us
  local copies, waits for them, and re-layouts: 9.12 us -> 0 us
  matrix products: 5.71 us -> 0 us
    pallas_call x2 -> x1, Pallas kernels: 159 us -> 142 us  [run_layer(): pl.pallas_call(functools.partial(layer_kernel, sp_size, dp_size, head_siz...]
    unnamed x17 -> x0, local copies, waits for them, and re-layouts: 6.65 us -> none
    dot_general x3 -> x0, matrix products: 5.71 us -> none  [the longest x2 3.58 us: shards(): picked = jnp.dot(select, returned, preferred_element_type=jnp.float32)]
    broadcast_in_dim x0 -> x1, other arithmetic: none -> 2.09 us  [shards(): return total.astype(jnp.bfloat16)[None]]
where the time goes in v1:
time: 144 us
  Pallas kernels  142 us (99%)
  other arithmetic  2.09 us (1%)
    pallas_call x1, Pallas kernels, run_layer(): pl.pallas_call(functools.partial(layer_kernel, sp_size, dp_size, head_siz...  142 us

profile of v1, /device:TPU:0, one launch (start us, length us, event | category | flops | bytes accessed | tf_op | source)
XLA Modules:
  0.0 143.9 jit_solution(11466009069688314420)
XLA Ops:
  0.0 141.8 %layer.1 = f32[128,2048]{1,0:T(8,128)} custom-call(bf16[128,2048]{1,0:T(8,128)(2,1)} %bitcast.22, bf16[128,2048]{1,0:T(8,128)(2,1)} %bitcast.23, bf16[128,2048]{1,0:T(8,128)(2,1)} %bitcast.24, bf16[2048,512]{1,0:T(8,128)(2,1)} %refs_3_.1, bf16[128,2048]{1,0:T(8,128)(2,1)} %bitcast.25, bf16[2048,1024]{1,0:T(8,128)(2,1)} %bitcast.19, ...), custom_call_target="tpu_custom_call" | custom-call | tf_op jit(solution)/shard_map/layer/pallas_call | solution.py:556
  141.8 2.1 %convert_bitcast_fusion = bf16[1,128,2048]{2,1,0:T(8,128)(2,1)} fusion(f32[128,2048]{1,0:T(8,128)} %layer.1), kind=kLoop, calls=%fused_computation | loop fusion | flops 262144 | bytes 1572864 | tf_op jit(solution)/shard_map/broadcast_in_dim | solution.py:595

commit v2 on v1

--- a/solution.py
+++ b/solution.py
@@ -13,6 +13,7 @@
 MESH = pl.DeviceIdType.MESH
 LANES = 128
 BLOCK = 256
+DEPTH = 4
 
 
 def place(index, size):
@@ -38,6 +39,7 @@
     q_buf, k_buf, v_buf, q_norm, k_head, v_ones, o_buf,
     local_sem, send_sem, recv_sem, own_sem, back_send, back_recv,
     weight_sem, weight_send, weight_recv, pass_send, pass_recv, resid_sem,
+    spread_send, spread_recv,
 ):
     me = lax.axis_index("sp")
     column = lax.axis_index("dp")
@@ -49,18 +51,42 @@
     inner = LANES // head_size
     sources, buffers = (q_ref, k_ref, v_ref), (q_buf, k_buf, v_buf)
 
-    def weight_across(step):
-        return pltpu.make_async_remote_copy(
-            src_ref=weight_ref,
-            dst_ref=weights.at[column],
-            send_sem=weight_send.at[step],
-            recv_sem=weight_recv.at[step],
+    width_x = n // DEPTH
+    x, plane_x = me % width_x, me - me % width_x
+    rows = weight_ref.shape[0]
+    share = rows // 2 // width_x
+
+    def weight_rows(part):
+        if part is None:
+            return pl.ds(0, rows // 2)
+        return pl.ds(pl.multiple_of(rows // 2 + part * share, share), share)
+
+    def weight_block(step):
+        return lax.rem(row_y + rows_y - step, rows_y) * 2 + core
+
+    def weight_across(step, part, kind):
+        return pltpu.make_async_remote_copy(
+            src_ref=weight_ref.at[weight_rows(part), :],
+            dst_ref=weights.at[column, weight_rows(part), :],
+            send_sem=weight_send.at[kind, step],
+            recv_sem=weight_recv.at[kind, step],
             device_id={"dp": lax.rem(row_y + step, rows_y) * 2 + core},
             device_id_type=MESH,
         )
 
+    def weight_spread(step, turn, part):
+        piece = weights.at[weight_block(step), weight_rows(part), :]
+        return pltpu.make_async_remote_copy(
+            src_ref=piece,
+            dst_ref=piece,
+            send_sem=spread_send.at[step, turn],
+            recv_sem=spread_recv.at[step, turn],
+            device_id={"sp": plane_x + lax.rem(x + turn, width_x)},
+            device_id_type=MESH,
+        )
+
     def weight_pass(step):
-        block = lax.rem(row_y + rows_y - step, rows_y) * 2 + core
+        block = weight_block(step)
         return pltpu.make_async_remote_copy(
             src_ref=weight_ref if step == 0 else weights.at[block],
             dst_ref=weights.at[block],
@@ -77,10 +103,17 @@
         return pltpu.make_async_remote_copy(
             src_ref=sources[kind].at[:, place(target * pairs + pair, LANES)],
             dst_ref=buffers[kind].at[pair, place(me, tok), :],
-            send_sem=send_sem.at[kind, pair, step],
-            recv_sem=recv_sem.at[kind, pair, step],
+            send_sem=send_sem.at[kind],
+            recv_sem=recv_sem.at[kind, pair],
             device_id={"sp": target},
             device_id_type=MESH,
+        )
+
+    def every_outgoing(kind, pair):
+        view = buffers[kind].at[pair, pl.ds(0, (n - 1) * tok), :]
+        return pltpu.make_async_remote_copy(
+            src_ref=view, dst_ref=view, send_sem=send_sem.at[kind],
+            recv_sem=recv_sem.at[kind, pair], device_id={"dp": twin}, device_id_type=MESH,
         )
 
     def own(kind, pair):
@@ -90,13 +123,12 @@
             local_sem.at[kind, pair],
         )
 
-    def backward(pair, step):
-        target = lax.rem(me + step, n)
-        return pltpu.make_async_remote_copy(
-            src_ref=o_buf.at[pair, place(target, tok), :],
+    def backward(pair, target):
+        return pltpu.make_async_remote_copy(
+            src_ref=o_buf.at[pair, pl.ds(target * tok, tok), :],
             dst_ref=out_ref.at[:, place(me * pairs + pair, LANES)],
-            send_sem=back_send.at[pair, step],
-            recv_sem=back_recv.at[pair, step],
+            send_sem=back_send,
+            recv_sem=back_recv,
             device_id={"sp": target},
             device_id_type=MESH,
         )
@@ -116,7 +148,9 @@
             own(kind, pair).start()
 
     for step in range(1, rows_y):
-        weight_across(step).start()
+        weight_across(step, x, 0).start()
+    for step in range(1, rows_y):
+        weight_across(step, None, 1).start()
     weight_pass(0).start()
     weight_own.start()
     load_resid = pltpu.make_async_copy(resid_ref, resid_buf, resid_sem)
@@ -144,8 +178,7 @@
     def one_pair(pair, carry):
         for kind in range(3):
             own(kind, pair).wait()
-            for step in range(1, n):
-                outgoing(kind, pair, step).wait_recv()
+            every_outgoing(kind, pair).wait_recv()
         floats = q_buf[pair].astype(jnp.float32)
         floats = floats * lax.rsqrt(half_means(floats * floats, head_size) + EPS)
         normed = (floats * q_gain).astype(jnp.bfloat16)
@@ -189,28 +222,50 @@
                 result = total[:, :LANES] / total[:, LANES:]
                 merged = result if head == 0 else jnp.where(out_lane == head, result, merged)
             o_buf[pair, here, :] = merged.astype(jnp.bfloat16)
-        for step in range(1, n):
-            backward(pair, step).start()
-        own_back(pair).start()
+            for target in range(first // tok, (first + BLOCK) // tok):
+                @pl.when(target == me)
+                def _():
+                    own_back(pair).start()
+
+                @pl.when(target != me)
+                def _():
+                    backward(pair, target).start()
+
+        @pl.when(pair == 0)
+        def _():
+            for step in range(1, rows_y):
+                weight_across(step, x, 0).wait_recv()
+                for turn in range(1, width_x):
+                    weight_spread(step, turn, x).start()
+
         return carry
 
     lax.fori_loop(0, pairs, one_pair, 0)
     for step in range(1, rows_y):
-        weight_across(step).wait_recv()
+        weight_across(step, None, 1).wait_recv()
+        for turn in range(1, width_x):
+            weight_spread(step, turn, lax.rem(x + width_x - turn, width_x)).wait_recv()
         weight_pass(step).start()
 
     def finish(pair, carry):
         own_back(pair).wait()
-        for step in range(1, n):
-            backward(pair, step).wait()
-            for kind in range(3):
-                outgoing(kind, pair, step).wait_send()
+        for kind in range(3):
+            every_outgoing(kind, pair).wait_send()
         return carry
 
     lax.fori_loop(0, pairs, finish, 0)
+    every_back = pltpu.make_async_remote_copy(
+        src_ref=o_buf.at[:, pl.ds(0, (n - 1) * tok), :],
+        dst_ref=out_ref.at[:, pl.ds(0, (n - 1) * pairs * LANES)],
+        send_sem=back_send, recv_sem=back_recv, device_id={"dp": twin}, device_id_type=MESH,
+    )
+    every_back.wait()
     weight_own.wait()
     for step in range(1, rows_y):
-        weight_across(step).wait_send()
+        weight_across(step, x, 0).wait_send()
+        weight_across(step, None, 1).wait_send()
+        for turn in range(1, width_x):
+            weight_spread(step, turn, x).wait_send()
     for step in range(rows_y):
         weight_pass(step).wait()
     load_resid.wait()
@@ -305,8 +360,8 @@
         return pltpu.make_async_remote_copy(
             src_ref=packed.at[kind, target, :, columns(chunk)],
             dst_ref=arrived.at[kind, step, :, columns(chunk)],
-            send_sem=send_sem.at[kind, chunk, step],
-            recv_sem=recv_sem.at[kind, chunk, step],
+            send_sem=send_sem.at[kind],
+            recv_sem=recv_sem.at[kind, step // per],
             device_id=coords(side * half + target),
             device_id_type=MESH,
         )
@@ -316,10 +371,16 @@
         return pltpu.make_async_remote_copy(
             src_ref=result.at[kind, step, :, columns(chunk)],
             dst_ref=returned.at[kind, seat, :, columns(chunk)],
-            send_sem=back_send.at[kind, chunk, step],
-            recv_sem=back_recv.at[kind, chunk, step],
+            send_sem=back_send.at[kind],
+            recv_sem=back_recv.at[kind, chunk],
             device_id=coords(side * half + target),
             device_id_type=MESH,
+        )
+
+    def dummy(view, sent, received):
+        return pltpu.make_async_remote_copy(
+            src_ref=view, dst_ref=view, send_sem=sent, recv_sem=received,
+            device_id=coords(twin), device_id_type=MESH,
         )
 
     def sum_copy(chunk):
@@ -362,11 +423,16 @@
         def group(index, carry):
             first = index * per
 
-            def take(step):
-                for chunk in range(CHUNKS):
-                    outgoing(kind, step, chunk).wait_recv()
-
-            others(take, first, first + per)
+            sent, received = send_sem.at[kind], recv_sem.at[kind, index]
+
+            @pl.when(first == mine)
+            def _():
+                dummy(arrived.at[kind, pl.ds(first + 1, per - 1)], sent, received).wait_recv()
+
+            @pl.when(first != mine)
+            def _():
+                dummy(arrived.at[kind, pl.ds(first, per)], sent, received).wait_recv()
+
             rows = arrived[kind, pl.ds(first, per)].reshape(per * cap, width)
             gate = jnp.dot(rows, gate_buf[...], preferred_element_type=jnp.float32)
             upper = jnp.dot(rows, up_buf[...], preferred_element_type=jnp.float32)
@@ -401,7 +467,8 @@
         return picks
 
     def combine(kind, picks, chunk):
-        others(lambda step: backward(kind, step, chunk).wait_recv())
+        view = returned.at[kind, pl.ds(0, half - 1), :, columns(chunk)]
+        dummy(view, back_send.at[kind], back_recv.at[kind, chunk]).wait_recv()
         block = returned[kind, :, :, columns(chunk)].reshape(half * cap, part)
         total = None
         for pick, weight in picks:
@@ -440,13 +507,10 @@
         row_copies[chunk].wait_send()
         sum_copy(chunk).wait_send()
 
-    def drain(step):
-        for kind in range(2):
-            for chunk in range(CHUNKS):
-                outgoing(kind, step, chunk).wait_send()
-                backward(kind, step, chunk).wait_send()
-
-    others(drain)
+    for kind in range(2):
+        whole = pl.ds(0, half - 1)
+        dummy(packed.at[kind, whole], send_sem.at[kind], recv_sem.at[kind, 0]).wait_send()
+        dummy(result.at[kind, whole], back_send.at[kind], back_recv.at[kind, 0]).wait_send()
 
 
 def layer_kernel(sp_size, dp_size, head_size, per, top, *refs):
@@ -457,7 +521,7 @@
     small = scratch[:7]
     gate_buf, up_buf, down_buf, mid_ref, normed_ref, info_ref = scratch[7:13]
     small_sem, load_sem = scratch[13:15]
-    attention_scratch, expert_scratch = scratch[15:37], scratch[37:]
+    attention_scratch, expert_scratch = scratch[15:39], scratch[39:]
     small_loads = [
         pltpu.make_async_copy(source, target, small_sem.at[index])
         for index, (source, target) in enumerate(zip(inputs[8:], small))
@@ -509,7 +573,7 @@
     n = sp_size * dp_size
     half = n // 2
     cap = 2 * tok * top // n
-    per = max(1, min(half, LANES // cap))
+    per = max(1, min(half // 2, LANES // cap))
     small = (decay, query_gain, key_gain, norm_gain, routes, group_weight, inner_share)
     dma = pltpu.SemaphoreType.DMA
     rows = pltpu.VMEM((tok, width), jnp.bfloat16)
@@ -517,7 +581,6 @@
     head_pairs = pltpu.VMEM((pairs, length, LANES), jnp.bfloat16)
     blocks = pltpu.VMEM((2, half, cap, width), jnp.bfloat16)
     sums = pltpu.VMEM((CHUNKS, tok, width // CHUNKS), jnp.bfloat16)
-    flags = dma((2, CHUNKS, half))
     chunk_flags = dma((CHUNKS,))
     scratch = [pltpu.VMEM(array.shape, array.dtype) for array in small]
     scratch += [pltpu.VMEM(array.shape, array.dtype) for array in (gate, upper, down)]
@@ -534,22 +597,24 @@
         pltpu.VMEM((length, 2 * LANES), jnp.bfloat16),
         head_pairs,
         dma((3, pairs)),
-        dma((3, pairs, sp_size)),
-        dma((3, pairs, sp_size)),
+        dma((3,)),
+        dma((3, pairs)),
         dma((pairs,)),
-        dma((pairs, sp_size)),
-        dma((pairs, sp_size)),
         dma,
-        dma((dp_size,)),
-        dma((dp_size,)),
-        dma((dp_size,)),
-        dma((dp_size,)),
         dma,
+        dma,
+        dma((2, dp_size // 2)),
+        dma((2, dp_size // 2)),
+        dma((dp_size // 2,)),
+        dma((dp_size // 2,)),
+        dma,
+        dma((dp_size // 2, sp_size // DEPTH)),
+        dma((dp_size // 2, sp_size // DEPTH)),
     ]
     expert_scratch = [
         rows, info, blocks, blocks, blocks, blocks, sums, sums,
         dma((2,)), chunk_flags, chunk_flags,
-        flags, flags, flags, flags,
+        dma((2,)), dma((2, half // per)), dma((2,)), dma((2, CHUNKS)),
         chunk_flags, chunk_flags,
     ]
     in_hbm = pl.BlockSpec(memory_space=pltpu.HBM)

time: 144 us -> 135 us (0.938)
  Pallas kernels: 142 us -> 132 us
    pallas_call x1, Pallas kernels: 142 us -> 132 us  [run_layer(): pl.pallas_call(functools.partial(layer_kernel, sp_size, dp_size, head_siz...]
where the time goes in v2:
time: 135 us; the launch traced here: 134 us
  Pallas kernels  132 us (98%)
  other arithmetic  2.09 us (2%)
    pallas_call x1, Pallas kernels, run_layer(): pl.pallas_call(functools.partial(layer_kernel, sp_size, dp_size, head_siz...  132 us

profile of v2, /device:TPU:0, one launch (start us, length us, event | category | flops | bytes accessed | tf_op | source)
XLA Modules:
  0.0 134.5 jit_solution(17854826688165718638)
XLA Ops:
  0.0 132.4 %layer.1 = f32[128,2048]{1,0:T(8,128)} custom-call(bf16[128,2048]{1,0:T(8,128)(2,1)} %bitcast.22, bf16[128,2048]{1,0:T(8,128)(2,1)} %bitcast.23, bf16[128,2048]{1,0:T(8,128)(2,1)} %bitcast.24, bf16[2048,512]{1,0:T(8,128)(2,1)} %refs_3_.1, bf16[128,2048]{1,0:T(8,128)(2,1)} %bitcast.25, bf16[2048,1024]{1,0:T(8,128)(2,1)} %bitcast.19, ...), custom_call_target="tpu_custom_call" | custom-call | tf_op jit(solution)/shard_map/layer/pallas_call | solution.py:621
  132.4 2.1 %convert_bitcast_fusion = bf16[1,128,2048]{2,1,0:T(8,128)(2,1)} fusion(f32[128,2048]{1,0:T(8,128)} %layer.1), kind=kLoop, calls=%fused_computation | loop fusion | flops 262144 | bytes 1572864 | tf_op jit(solution)/shard_map/broadcast_in_dim | solution.py:660

commit v3 on v2

--- a/solution.py
+++ b/solution.py
@@ -32,11 +32,11 @@
 
 
 def attention_stage(
-    n, dp_size, head_size, small_loads, weight_loads,
+    n, dp_size, head_size, weight_loads,
     q_ref, k_ref, v_ref, weight_ref, resid_ref,
     decay_ref, q_gain_ref, k_gain_ref, norm_gain_ref, routes_ref, group_ref, share_ref,
     mid_ref, normed_ref, info_ref, out_ref, weights, resid_buf,
-    q_buf, k_buf, v_buf, q_norm, k_head, v_ones, o_buf,
+    q_buf, k_buf, v_buf, k_head, v_ones, o_buf,
     local_sem, send_sem, recv_sem, own_sem, back_send, back_recv,
     weight_sem, weight_send, weight_recv, pass_send, pass_recv, resid_sem,
     spread_send, spread_recv,
@@ -157,17 +157,11 @@
     load_resid.start()
     for load in weight_loads:
         load.start()
-    for load in small_loads:
-        load.wait()
     info_ref[...] = routing_info(routes_ref, group_ref, share_ref, n * dp_size)
-    q_gain = jnp.concatenate([q_gain_ref[...]] * inner, axis=1)
-    k_gain = jnp.concatenate([k_gain_ref[...]] * inner, axis=1)
-
     row = lax.broadcasted_iota(jnp.int32, (BLOCK, BLOCK), 0)
     col = lax.broadcasted_iota(jnp.int32, (BLOCK, BLOCK), 1)
     lane = lax.broadcasted_iota(jnp.int32, (length, LANES), 1) // head_size
     out_lane = lax.broadcasted_iota(jnp.int32, (BLOCK, LANES), 1) // head_size
-    scale = head_size ** (-0.5)
     v_ones[:, LANES:] = jnp.ones((length, LANES), jnp.bfloat16)
 
     def scores_of(queries, keys):
@@ -179,20 +173,14 @@
         for kind in range(3):
             own(kind, pair).wait()
             every_outgoing(kind, pair).wait_recv()
-        floats = q_buf[pair].astype(jnp.float32)
-        floats = floats * lax.rsqrt(half_means(floats * floats, head_size) + EPS)
-        normed = (floats * q_gain).astype(jnp.bfloat16)
-        q_norm[...] = (normed.astype(jnp.float32) * scale).astype(jnp.bfloat16)
         floats = k_buf[pair].astype(jnp.float32)
-        floats = floats * lax.rsqrt(half_means(floats * floats, head_size) + EPS)
-        floats = floats * k_gain
         for head in range(inner):
             k_head[head] = jnp.where(lane == head, floats, 0.0).astype(jnp.bfloat16)
         v_ones[:, :LANES] = v_buf[pair]
         for block in range(length // BLOCK):
             first = block * BLOCK
             here = slice(first, first + BLOCK)
-            query_block = q_norm[here, :]
+            query_block = q_buf[pair, here, :]
             merged = None
             for head in range(inner):
                 decay = decay_ref[pl.ds(pair * inner + head, 1), :]
@@ -500,7 +488,8 @@
         total = combine(0, picks, chunk)
         sum_copy(chunk).wait_recv()
         total = total + incoming[chunk].astype(jnp.float32)
-        out_ref[:, columns(chunk)] = mid_ref[:, columns(chunk)].astype(jnp.float32) + total
+        total = total + mid_ref[:, columns(chunk)].astype(jnp.float32)
+        out_ref[:, columns(chunk)] = total.astype(jnp.bfloat16)
 
     info_copy.wait_send()
     for chunk in range(CHUNKS):
@@ -521,7 +510,12 @@
     small = scratch[:7]
     gate_buf, up_buf, down_buf, mid_ref, normed_ref, info_ref = scratch[7:13]
     small_sem, load_sem = scratch[13:15]
-    attention_scratch, expert_scratch = scratch[15:39], scratch[39:]
+    attention_scratch, expert_scratch = scratch[15:38], scratch[38:-5]
+    q_raw, k_raw, q_src, k_src, stage_sem = scratch[-5:]
+    stage_loads = [
+        pltpu.make_async_copy(source, target, stage_sem.at[index])
+        for index, (source, target) in enumerate(((q_ref, q_raw), (k_ref, k_raw)))
+    ]
     small_loads = [
         pltpu.make_async_copy(source, target, small_sem.at[index])
         for index, (source, target) in enumerate(zip(inputs[8:], small))
@@ -532,7 +526,7 @@
             ((gate_ref, gate_buf), (up_ref, up_buf), (down_ref, down_buf))
         )
     ]
-    for load in small_loads:
+    for load in stage_loads + small_loads:
         load.start()
     n = sp_size * dp_size
     me = lax.axis_index("sp") * dp_size + lax.axis_index("dp")
@@ -547,10 +541,29 @@
         return carry
 
     lax.fori_loop(1, n, greet, 0)
+    for load in stage_loads + small_loads:
+        load.wait()
+    q_gain = jnp.concatenate([small[1][...]] * (LANES // head_size), axis=1)
+    k_gain = jnp.concatenate([small[2][...]] * (LANES // head_size), axis=1)
+
+    def norm_columns(block, carry):
+        here = place(block, LANES)
+        for raw, normed, gain, scale in (
+            (q_raw, q_src, q_gain, head_size ** (-0.5)), (k_raw, k_src, k_gain, 1.0),
+        ):
+            floats = raw[:, here].astype(jnp.float32)
+            floats = floats * lax.rsqrt(half_means(floats * floats, head_size) + EPS)
+            rounded = (floats * gain).astype(jnp.bfloat16)
+            if scale != 1.0:
+                rounded = (rounded.astype(jnp.float32) * scale).astype(jnp.bfloat16)
+            normed[:, here] = rounded
+        return carry
+
+    lax.fori_loop(0, q_raw.shape[1] // LANES, norm_columns, 0)
     pl.semaphore_wait(barrier, n - 1)
     attention_stage(
-        sp_size, dp_size, head_size, small_loads, weight_loads,
-        q_ref, k_ref, v_ref, weight_ref, resid_ref, *small,
+        sp_size, dp_size, head_size, weight_loads,
+        q_src, k_src, v_ref, weight_ref, resid_ref, *small,
         mid_ref, normed_ref, info_ref, *attention_scratch,
     )
     expert_stage(
@@ -592,7 +605,6 @@
         head_pairs,
         head_pairs,
         head_pairs,
-        pltpu.VMEM((length, LANES), jnp.bfloat16),
         pltpu.VMEM((inner, length, LANES), jnp.bfloat16),
         pltpu.VMEM((length, 2 * LANES), jnp.bfloat16),
         head_pairs,
@@ -616,11 +628,12 @@
         dma((2,)), chunk_flags, chunk_flags,
         dma((2,)), dma((2, half // per)), dma((2,)), dma((2, CHUNKS)),
         chunk_flags, chunk_flags,
+        rows, rows, rows, rows, dma((2,)),
     ]
     in_hbm = pl.BlockSpec(memory_space=pltpu.HBM)
     return pl.pallas_call(
         functools.partial(layer_kernel, sp_size, dp_size, head_size, per, top),
-        out_shape=jax.ShapeDtypeStruct((tok, width), jnp.float32),
+        out_shape=jax.ShapeDtypeStruct((tok, width), jnp.bfloat16),
         in_specs=[in_hbm] * 15,
         out_specs=pl.BlockSpec(memory_space=pltpu.VMEM),
         scratch_shapes=scratch + attention_scratch + expert_scratch,
@@ -657,7 +670,7 @@
         forget_cache[0], query_gain[None], key_gain[None], norm_gain[None],
         routes[0].T, group_weight, inner_share[0].T,
     )
-    return total.astype(jnp.bfloat16)[None]
+    return total[None]
 
 
 def solution(mesh):

time: 135 us -> 133 us (0.985)
  other arithmetic: 2.09 us -> 0 us
  local copies, waits for them, and re-layouts: 0 us -> 1.88 us
    broadcast_in_dim x1 -> x0, other arithmetic: 2.09 us -> none  [shards(): return total.astype(jnp.bfloat16)[None]]
    unnamed x0 -> x1, local copies, waits for them, and re-layouts: none -> 1.88 us
where the time goes in v3:
time: 133 us
  Pallas kernels  131 us (98%)
  local copies, waits for them, and re-layouts  1.88 us (1%)
    pallas_call x1, Pallas kernels, run_layer(): pl.pallas_call(functools.partial(layer_kernel, sp_size, dp_size, head_siz...  131 us

profile of v3, /device:TPU:0, one launch (start us, length us, event | category | flops | bytes accessed | tf_op | source)
XLA Modules:
  0.0 133.1 jit_solution(310192215337705727)
XLA Ops:
  0.0 131.2 %layer.1 = bf16[128,2048]{1,0:T(8,128)(2,1)} custom-call(bf16[128,2048]{1,0:T(8,128)(2,1)} %bitcast.22, bf16[128,2048]{1,0:T(8,128)(2,1)} %bitcast.23, bf16[128,2048]{1,0:T(8,128)(2,1)} %bitcast.24, bf16[2048,512]{1,0:T(8,128)(2,1)} %refs_3_.1, bf16[128,2048]{1,0:T(8,128)(2,1)} %bitcast.25, bf16[2048,1024]{1,0:T(8,128)(2,1)} %bitcast.18, ...), custom_call_target="tpu_custom_call" | custom-call | tf_op jit(solution)/shard_map/layer/pallas_call | solution.py:634
  131.2 1.9 %copy.17 = bf16[1,128,2048]{2,1,0:T(8,128)(2,1)} copy(bf16[1,128,2048]{2,1,0:T(8,128)(2,1)} %bitcast.21) | data formatting | bytes 1048576

commit v4 on v3

--- a/solution.py
+++ b/solution.py
@@ -31,8 +31,30 @@
     return total * (1.0 / head_size)
 
 
+def far_row_copy(normed_ref, far_rows, row_send, row_recv, columns, chunk):
+    half_line = lax.axis_size("sp") // 2
+    line = lax.rem(lax.axis_index("sp") + half_line, 2 * half_line)
+    return pltpu.make_async_remote_copy(
+        src_ref=normed_ref.at[:, columns],
+        dst_ref=far_rows.at[:, columns],
+        send_sem=row_send.at[chunk],
+        recv_sem=row_recv.at[chunk],
+        device_id={"sp": line},
+        device_id_type=MESH,
+    )
+
+
+def far_info_copy(info_ref, far_info, info_sem):
+    half_line = lax.axis_size("sp") // 2
+    line = lax.rem(lax.axis_index("sp") + half_line, 2 * half_line)
+    return pltpu.make_async_remote_copy(
+        src_ref=info_ref, dst_ref=far_info, send_sem=info_sem.at[0], recv_sem=info_sem.at[1],
+        device_id={"sp": line}, device_id_type=MESH,
+    )
+
+
 def attention_stage(
-    n, dp_size, head_size, weight_loads,
+    n, dp_size, head_size, weight_loads, send_rows,
     q_ref, k_ref, v_ref, weight_ref, resid_ref,
     decay_ref, q_gain_ref, k_gain_ref, norm_gain_ref, routes_ref, group_ref, share_ref,
     mid_ref, normed_ref, info_ref, out_ref, weights, resid_buf,
@@ -158,6 +180,7 @@
     for load in weight_loads:
         load.start()
     info_ref[...] = routing_info(routes_ref, group_ref, share_ref, n * dp_size)
+    send_rows(0)
     row = lax.broadcasted_iota(jnp.int32, (BLOCK, BLOCK), 0)
     col = lax.broadcasted_iota(jnp.int32, (BLOCK, BLOCK), 1)
     lane = lax.broadcasted_iota(jnp.int32, (length, LANES), 1) // head_size
@@ -273,6 +296,7 @@
         columns = slice(block * span, (block + 1) * span)
         scaled = mid_ref[:, columns].astype(jnp.float32) * factor
         normed_ref[:, columns] = (scaled * norm_gain_ref[:, columns]).astype(jnp.bfloat16)
+        send_rows((block + 1) * span)
 
 
 INFO_ROWS = 8
@@ -325,37 +349,27 @@
         return slice(chunk * part, (chunk + 1) * part)
 
     def coords(flat):
-        return {"sp": flat // dp_size, "dp": flat % dp_size}
-
-    info_copy = pltpu.make_async_remote_copy(
-        src_ref=info_ref, dst_ref=far_info, send_sem=info_sem.at[0], recv_sem=info_sem.at[1],
-        device_id=coords(twin), device_id_type=MESH,
-    )
+        return {"sp": lax.div(flat, dp_size), "dp": lax.rem(flat, dp_size)}
+
+    info_copy = far_info_copy(info_ref, far_info, info_sem)
     row_copies = [
-        pltpu.make_async_remote_copy(
-            src_ref=normed_ref.at[:, columns(chunk)],
-            dst_ref=far_rows.at[:, columns(chunk)],
-            send_sem=row_send.at[chunk],
-            recv_sem=row_recv.at[chunk],
-            device_id=coords(twin),
-            device_id_type=MESH,
-        )
+        far_row_copy(normed_ref, far_rows, row_send, row_recv, columns(chunk), chunk)
         for chunk in range(CHUNKS)
     ]
 
     def outgoing(kind, step, chunk):
-        target = (seat + mine + step) % half
+        target = lax.rem(seat + mine + step, half)
         return pltpu.make_async_remote_copy(
             src_ref=packed.at[kind, target, :, columns(chunk)],
             dst_ref=arrived.at[kind, step, :, columns(chunk)],
             send_sem=send_sem.at[kind],
-            recv_sem=recv_sem.at[kind, step // per],
+            recv_sem=recv_sem.at[kind, lax.div(step, per)],
             device_id=coords(side * half + target),
             device_id_type=MESH,
         )
 
     def backward(kind, step, chunk):
-        target = (seat + half + half - mine - step) % half
+        target = lax.rem(seat + half + half - mine - step, half)
         return pltpu.make_async_remote_copy(
             src_ref=result.at[kind, step, :, columns(chunk)],
             dst_ref=returned.at[kind, seat, :, columns(chunk)],
@@ -464,9 +478,6 @@
             total = term if total is None else total + term
         return total
 
-    info_copy.start()
-    for copy in row_copies:
-        copy.start()
     for chunk in range(CHUNKS):
         dispatch(0, normed_ref, info_ref, chunk)
     info_copy.wait_recv()
@@ -561,8 +572,19 @@
 
     lax.fori_loop(0, q_raw.shape[1] // LANES, norm_columns, 0)
     pl.semaphore_wait(barrier, n - 1)
+    far_rows, row_send, row_recv = expert_scratch[0], expert_scratch[9], expert_scratch[10]
+
+    def send_rows(done):
+        width = normed_ref.shape[1]
+        part = width // CHUNKS
+        if done == 0:
+            far_info_copy(info_ref, expert_scratch[1], expert_scratch[8]).start()
+        elif done % part == 0:
+            columns, chunk = slice(done - part, done), done // part - 1
+            far_row_copy(normed_ref, far_rows, row_send, row_recv, columns, chunk).start()
+
     attention_stage(
-        sp_size, dp_size, head_size, weight_loads,
+        sp_size, dp_size, head_size, weight_loads, send_rows,
         q_src, k_src, v_ref, weight_ref, resid_ref, *small,
         mid_ref, normed_ref, info_ref, *attention_scratch,
     )

time: 133 us -> 133 us (level)
  no operation moved by 1% of the time
where the time goes in v4:
time: 133 us; the launch traced here: 132 us
  Pallas kernels  130 us (98%)
  local copies, waits for them, and re-layouts  1.88 us (1%)
    pallas_call x1, Pallas kernels, run_layer(): pl.pallas_call(functools.partial(layer_kernel, sp_size, dp_size, head_siz...  130 us

profile of v4, /device:TPU:0, one launch (start us, length us, event | category | flops | bytes accessed | tf_op | source)
XLA Modules:
  0.0 132.3 jit_solution(17544681442566030106)
XLA Ops:
  0.0 130.5 %layer.1 = bf16[128,2048]{1,0:T(8,128)(2,1)} custom-call(bf16[128,2048]{1,0:T(8,128)(2,1)} %bitcast.22, bf16[128,2048]{1,0:T(8,128)(2,1)} %bitcast.23, bf16[128,2048]{1,0:T(8,128)(2,1)} %bitcast.24, bf16[2048,512]{1,0:T(8,128)(2,1)} %refs_3_.1, bf16[128,2048]{1,0:T(8,128)(2,1)} %bitcast.25, bf16[2048,1024]{1,0:T(8,128)(2,1)} %bitcast.18, ...), custom_call_target="tpu_custom_call" | custom-call | tf_op jit(solution)/shard_map/layer/pallas_call | solution.py:656
  130.5 1.9 %copy.17 = bf16[1,128,2048]{2,1,0:T(8,128)(2,1)} copy(bf16[1,128,2048]{2,1,0:T(8,128)(2,1)} %bitcast.21) | data formatting | bytes 1048576
